TPU v7x, 32 devices: a whole 2x2x4 slice. The times are simulated.
32 devices in a mesh: ep: 16 (over z, y, core), tp: 2 (over x).
Axes of the slice: x: 2, y: 2, z: 4, core: 2. Of those that a mesh axis runs over, the one named last changes fastest.
Arguments:
- tokens: bfloat16 [128, 1024], P(('ep', 'tp')), may hold values from -6 to 6
- lengths: int32 [128], P(('ep', 'tp')), may hold values from 256 to 1024, as said below
- cache_latent: bfloat16 [128, 1024, 256], P(('ep', 'tp')), may hold values from -160 to 160
- cache_rope: bfloat16 [128, 32, 1024], P(('ep', 'tp')), may hold values from -6 to 6
- attn_gain: float32 [1024], replicated, may hold values from 0.1 to 1.9
- latent_gain: float32 [256], replicated, may hold values from 0.1 to 1.9
- post_gain: float32 [1024], replicated, may hold values from 0.1 to 1.9
- ffn_gain: float32 [1024], replicated, may hold values from 0.1 to 1.9
- out_gain: float32 [1024], replicated, may hold values from 0.1 to 1.9
- w_latent: bfloat16 [1024, 256], P(None, 'tp'), may hold values from -0.1875 to 0.1875
- w_rope_key: bfloat16 [1024, 32], replicated, may hold values from -0.1875 to 0.1875
- w_query: bfloat16 [1024, 768], P(None, 'tp'), may hold values from -0.1875 to 0.1875
- w_absorb_key: bfloat16 [8, 64, 256], P('tp'), may hold values from -0.75 to 0.75
- w_absorb_value: bfloat16 [8, 256, 64], P('tp'), may hold values from -0.375 to 0.375
- w_out: bfloat16 [512, 1024], P('tp'), may hold values from -0.25 to 0.25
- routes: int32 [128, 6], P(('ep', 'tp')), may hold values from 0 to 15, all different within a row; in each aligned block of 8 rows (0 to 7, 8 to 15, ...) at most 5 rows name the same one
- route_weights: float32 [128, 6], P(('ep', 'tp')), may hold values from 0.2 to 1
- w_exp_gate: bfloat16 [16, 1024, 256], P('ep'), may hold values from -0.1875 to 0.1875
- w_exp_up: bfloat16 [16, 1024, 256], P('ep'), may hold values from -0.1875 to 0.1875
- w_exp_down: bfloat16 [16, 256, 1024], P('ep'), may hold values from -0.375 to 0.375
- w_dense_gate: bfloat16 [4096, 1024], P('ep'), may hold values from -0.1875 to 0.1875
- w_dense_up: bfloat16 [4096, 1024], P('ep'), may hold values from -0.1875 to 0.1875
- w_dense_down: bfloat16 [4096, 1024], P('ep'), may hold values from -0.09375 to 0.09375
- dense_gate_vector: float32 [1024], replicated, may hold values from -0.1875 to 0.1875
Outputs:
- output: bfloat16 [128, 1024], P(('ep', 'tp'))
- new_latent: bfloat16 [128, 256], P(('ep', 'tp'))
- new_rope_key: bfloat16 [128, 32], P(('ep', 'tp'))
Inputs may be any that keep to these rules, and one draw needn't show every extreme that they name: `routes`: in each aligned block of 8 rows no expert is named by more than 5 rows; each row names 6 different experts. `lengths`: some sequence holds exactly 1024 cached positions.
All inputs are finite; a program needn't handle non-finite values.
Results may differ from a plain program's by a relative error of at most 0.015.
Values may be sent and summed in bfloat16 or wider, within the bound.
A program may use at most 64 MiB of HBM per device.

v0:
```python
import functools

import jax
import jax.numpy as jnp
import numpy as np
from jax import lax
from jax.experimental import pallas as pl
from jax.experimental.pallas import tpu as pltpu
from jax.sharding import PartitionSpec as P

epsilon = 1e-06
rope_base = 10000.0
negative = -1e30
MESH = pl.DeviceIdType.MESH
f32 = jnp.float32
bf16 = jnp.bfloat16

NAMES = (
    "tokens", "routes", "rweights", "coef_gain", "w_query", "w_latent",
    "w_abk", "w_rope", "lat_gain", "cache", "rope", "post_gain",
    "ffn_gain", "dvec", "weg", "weu", "wed", "wdg",
    "wdu", "wdd", "out_gain", "inverse",
)


def norm(values):
    return values * lax.rsqrt(jnp.mean(values * values, axis=-1, keepdims=True) + epsilon)


def dot(a, b):
    return jnp.dot(a, b, preferred_element_type=f32)


def dot_t(a, b):
    return lax.dot_general(a, b, (((1,), (1,)), ((), ())), preferred_element_type=f32)


def swap_halves(v):
    half = v.shape[1] // 2
    return jnp.concatenate([-v[:, half:], v[:, :half]], axis=1)


def silu(u):
    return u / (1.0 + jnp.exp(-u))


def kernel(ep, tp, *refs):
    n = len(NAMES)
    lengths = refs[0]
    hbm = dict(zip(NAMES, refs[1 : 1 + n]))
    wv_hbm, wo_hbm = refs[1 + n : 3 + n]
    out_ref, lat_ref, key_ref = refs[3 + n : 6 + n]
    scratch = refs[6 + n :]
    v = dict(zip(NAMES, scratch[:n]))
    (
        wv, wo, load_sem, tokbuf, qsend, qbuf, latsend, latbuf, att, coef, coefbuf,
        xown, xbuf, xrows, psend, pbuf,
        a_s, a_r, q_s, q_r, l_s, l_r, w1_s, w1_r, w2_s, w2_r, c_s, c_r, x_s, x_r, p_s, p_r,
    ) = scratch[n:]
    rows, width = v["tokens"].shape
    heads_local, nope, kv = v["w_abk"].shape
    rope_width = v["w_rope"].shape[0]
    span = nope + rope_width
    heads = heads_local * tp
    scaling = span ** (-0.5)
    me_e = lax.axis_index("ep")
    me_t = lax.axis_index("tp")
    core = lax.rem(me_e, 2)
    sibling = me_e + 1 - 2 * core

    loads = {}
    loads["wv"] = pltpu.make_async_copy(wv_hbm, wv.at[0], load_sem.at[n])
    loads["wo"] = pltpu.make_async_copy(wo_hbm, wo.at[0], load_sem.at[n + 1])
    loads["wv"].start()
    loads["wo"].start()
    for i, name in enumerate(NAMES):
        loads[name] = pltpu.make_async_copy(hbm[name], v[name], load_sem.at[i])
        loads[name].start()

    barrier = pltpu.get_barrier_semaphore()
    for k in range(1, tp):
        pl.semaphore_signal(
            barrier, inc=1, device_id={"tp": lax.rem(me_t + k, tp)}, device_id_type=MESH
        )
    for k in range(1, ep):
        pl.semaphore_signal(
            barrier, inc=1, device_id={"ep": lax.rem(me_e + k, ep)}, device_id_type=MESH
        )

    for name in ("tokens", "routes", "rweights", "inverse"):
        loads[name].wait()
    lane = lax.broadcasted_iota(jnp.int32, coef.shape, 1)
    total = jnp.zeros(coef.shape, f32)
    routes = v["routes"][...]
    rweights = v["rweights"][...]
    for k in range(routes.shape[1]):
        total = total + jnp.where(routes[:, k : k + 1] == lane, rweights[:, k : k + 1], 0.0)
    coef[...] = total

    def tables(count, per):
        row = lax.broadcasted_iota(jnp.int32, (count, rope_width), 0) // per
        pos = jnp.zeros((count, rope_width), jnp.int32)
        for s in range(rows):
            pos = jnp.where(row == s, lengths[s], pos)
        angles = pos.astype(f32) * v["inverse"][...]
        return jnp.cos(angles), jnp.sin(angles)

    cos_q, sin_q = tables(rows * heads, heads)
    cos_k, sin_k = tables(rows, 1)

    pl.semaphore_wait(barrier, (tp - 1) + (ep - 1))

    def remote(src, dst, ss, rs, where):
        return pltpu.make_async_remote_copy(
            src_ref=src, dst_ref=dst, send_sem=ss, recv_sem=rs, device_id=where,
            device_id_type=MESH,
        )

    back_t = [lax.rem(me_t + tp - k, tp) for k in range(tp)]
    ahead_t = [lax.rem(me_t + k, tp) for k in range(tp)]
    back_e = [lax.rem(me_e + ep - k, ep) for k in range(ep)]
    ahead_e = [lax.rem(me_e + k, ep) for k in range(ep)]
    a_copies = [
        remote(v["tokens"], tokbuf.at[k], a_s.at[k], a_r.at[k], {"tp": back_t[k]})
        for k in range(1, tp)
    ]
    for c in a_copies:
        c.start()
    half_h = heads_local // 2
    depth = wo.shape[1]
    quarter = depth // 8
    part = depth // 16

    def pieces(k):
        start = core * (4 * quarter)
        early = pl.ds(pl.multiple_of(start, quarter), 2 * quarter - part)
        late = pl.ds(pl.multiple_of(start + 2 * quarter - part, part), 2 * quarter + part)
        return (
            wv.at[k, pl.ds(core * half_h, half_h)],
            wo.at[k, early],
            wo.at[k, late],
        )

    w1 = [
        [
            remote(src, dst, w1_s.at[k, i], w1_r.at[k, i], {"tp": back_t[k]})
            for i, (src, dst) in enumerate(zip(pieces(0), pieces(k)))
        ]
        for k in range(1, tp)
    ]
    w2 = [
        [
            remote(dst, dst, w2_s.at[k, i], w2_r.at[k, i], {"ep": sibling})
            for i, dst in enumerate(pieces(k))
        ]
        for k in range(1, tp)
    ]
    loads['wv'].wait()
    loads['wo'].wait()
    for group in w1:
        group[0].start()
        group[1].start()
    c_copies = [
        remote(coef, coefbuf.at[k], c_s.at[k], c_r.at[k], {"ep": back_e[k]}) for k in range(1, ep)
    ]
    for c in c_copies:
        c.start()

    tokens = v["tokens"][...].astype(f32)
    for c in a_copies:
        c.wait_recv()
    everyone = jnp.concatenate(
        [tokens] + [tokbuf[k].astype(f32) for k in range(1, tp)], axis=0
    )
    loads["coef_gain"].wait()
    hidden = (norm(everyone) * v["coef_gain"][...]).astype(bf16)
    loads["w_query"].wait()
    queries = dot(hidden, v["w_query"][...]).astype(bf16).astype(f32)
    loads["w_latent"].wait()
    latent_part = dot(hidden, v["w_latent"][...])
    loads["w_abk"].wait()
    for h in range(heads_local):
        q_h = queries[:, h * span : h * span + nope].astype(bf16)
        ql = dot(q_h, v["w_abk"][h]).astype(bf16).astype(f32)
        qr = queries[:, h * span + nope : (h + 1) * span]
        for k in range(tp):
            for s in range(rows):
                r = k * rows + s
                target = qbuf if k == 0 else qsend
                target[k, s, h : h + 1, 0:kv] = ql[r : r + 1]
                target[k, s, h : h + 1, kv : kv + rope_width] = qr[r : r + 1]
    for k in range(1, tp):
        latsend[k] = latent_part[k * rows : (k + 1) * rows]
    latbuf[me_t] = latent_part[0:rows]
    q_copies = [
        remote(qsend.at[k], qbuf.at[tp - k], q_s.at[k], q_r.at[tp - k], {"tp": ahead_t[k]})
        for k in range(1, tp)
    ]
    l_copies = [
        remote(latsend.at[k], latbuf.at[me_t], l_s.at[k], l_r.at[tp - k], {"tp": ahead_t[k]})
        for k in range(1, tp)
    ]
    for c in q_copies + l_copies:
        c.start()
    for group in w1:
        group[2].start()
    loads["w_rope"].wait()
    raw_key = dot_t(hidden, v["w_rope"][...])[0:rows]
    new_key = (raw_key * cos_k + swap_halves(raw_key) * sin_k).astype(bf16)
    key_ref[...] = new_key
    loads["cache"].wait()
    loads["rope"].wait()
    loads["lat_gain"].wait()
    for c in q_copies + l_copies:
        c.wait_recv()
    for i in (0, 1):
        for group, forward in zip(w1, w2):
            group[i].wait_recv()
            forward[i].start()
    latent = jnp.concatenate([latbuf[t] for t in range(tp)], axis=1)
    new_latent = (norm(latent) * v["lat_gain"][...]).astype(bf16)
    lat_ref[...] = new_latent
    lat_f = new_latent.astype(f32)
    key_f = new_key.astype(f32)
    q_all = jnp.concatenate(
        [qbuf[k, s] for s in range(rows) for k in range(tp)], axis=0
    )
    q_lat = q_all[:, 0:kv]
    q_raw = q_all[:, kv : kv + rope_width]
    q_rot = (q_raw * cos_q + swap_halves(q_raw) * sin_q).astype(bf16)
    position = lax.broadcasted_iota(jnp.int32, (heads, v["cache"].shape[1]), 1)
    for s in range(rows):
        ql = q_lat[s * heads : (s + 1) * heads]
        qr = q_rot[s * heads : (s + 1) * heads]
        own = (
            jnp.sum(ql * lat_f[s : s + 1], axis=1, keepdims=True)
            + jnp.sum(qr.astype(f32) * key_f[s : s + 1], axis=1, keepdims=True)
        ) * scaling
        scores = (dot_t(ql.astype(bf16), v["cache"][s]) + dot(qr, v["rope"][s])) * scaling
        scores = jnp.where(position < lengths[s], scores, negative)
        top = jnp.maximum(jnp.max(scores, axis=1, keepdims=True), own)
        weights = jnp.exp(scores - top)
        own_weight = jnp.exp(own - top)
        share = 1.0 / (jnp.sum(weights, axis=1, keepdims=True) + own_weight)
        probabilities = (weights * share).astype(bf16)
        own_prob = (own_weight * share).astype(bf16).astype(f32)
        attended = dot(probabilities, v["cache"][s]) + own_prob * lat_f[s : s + 1]
        for j in range(kv // 128):
            att[j, s * heads : (s + 1) * heads] = attended[:, j * 128 : (j + 1) * 128]
    for group, forward in zip(w1, w2):
        group[2].wait_recv()
        forward[2].start()
    mixed = jnp.zeros((rows, width), f32)
    for k in range(tp):
        if k > 0:
            for c in w2[k - 1]:
                c.wait_recv()
        parts = []
        for h in range(heads_local):
            chosen = pl.ds(k * heads_local + h, rows, stride=heads)
            picked = jnp.concatenate([att[j, chosen, :] for j in range(kv // 128)], axis=1)
            parts.append(dot_t(picked.astype(bf16), wv[k, h]))
        head_out = jnp.concatenate(parts, axis=1).astype(bf16)
        mixed = mixed + dot(head_out, wo[k]).astype(bf16).astype(f32)
    loads["post_gain"].wait()
    loads["ffn_gain"].wait()
    residual = (tokens + norm(mixed) * v["post_gain"][...]).astype(bf16).astype(f32)
    ffn_in = (norm(residual) * v["ffn_gain"][...]).astype(bf16)
    xown[...] = ffn_in
    x_copies = [
        remote(xown, xbuf.at[k], x_s.at[k], x_r.at[k], {"ep": back_e[k]}) for k in range(1, ep)
    ]
    for c in x_copies:
        c.start()
    for name in ("dvec", "weg", "weu", "wed", "wdg", "wdu", "wdd", "out_gain"):
        loads[name].wait()
    lane_own = lax.broadcasted_iota(jnp.int32, coef.shape, 1) == me_e

    def own_weight_of(block):
        return jnp.sum(jnp.where(lane_own, block, 0.0), axis=1, keepdims=True)

    route_parts = [own_weight_of(coef[...])]
    for k in range(1, ep):
        c_copies[k - 1].wait_recv()
        route_parts.append(own_weight_of(coefbuf[k]))
    route_w = jnp.concatenate(route_parts, axis=0)
    xrows[0:rows] = ffn_in.astype(f32)
    for k in range(1, ep):
        x_copies[k - 1].wait_recv()
    for k in range(1, ep):
        xrows[k * rows : (k + 1) * rows] = xbuf[k].astype(f32)
    x_f = xrows[...]
    gate_of = 1.0 / (1.0 + jnp.exp(-jnp.sum(x_f * v["dvec"][...], axis=1, keepdims=True)))
    x = x_f.astype(bf16)
    act_e = (silu(dot(x, v["weg"][0])) * dot(x, v["weu"][0])).astype(bf16)
    act_d = (silu(dot_t(x, v["wdg"][...])) * dot_t(x, v["wdu"][...])).astype(bf16)
    partial = route_w * dot(act_e, v["wed"][0]).astype(bf16).astype(f32) + gate_of * dot(
        act_d, v["wdd"][...]
    )
    for k in range(1, ep):
        psend[k] = partial[k * rows : (k + 1) * rows].astype(bf16)
    p_copies = [
        remote(psend.at[k], pbuf.at[ep - k], p_s.at[k], p_r.at[ep - k], {"ep": ahead_e[k]})
        for k in range(1, ep)
    ]
    for c in p_copies:
        c.start()
    combined = partial[0:rows]
    for k in range(1, ep):
        p_copies[k - 1].wait_recv()
    for k in range(1, ep):
        combined = combined + pbuf[ep - k].astype(f32)
    out_ref[...] = (residual + norm(combined) * v["out_gain"][...]).astype(bf16)
    for c in a_copies + q_copies + l_copies + c_copies + x_copies + p_copies:
        c.wait_send()
    for group in w1 + w2:
        for c in group:
            c.wait_send()


def hand_over(*refs):
    half = len(refs) // 2
    for src, dst in zip(refs[:half], refs[half:]):
        dst[...] = src[...]


def shards(
    tokens, lengths, cache_latent, cache_rope, attn_gain, latent_gain, post_gain, ffn_gain,
    out_gain, w_latent, w_rope_key, w_query, w_absorb_key, w_absorb_value, w_out, routes,
    route_weights, w_exp_gate, w_exp_up, w_exp_down, w_dense_gate, w_dense_up, w_dense_down,
    dense_gate_vector,
):
    ep, tp = lax.axis_size("ep"), lax.axis_size("tp")
    rows, width = tokens.shape
    heads_local, _, kv = w_absorb_key.shape
    rope_width = w_rope_key.shape[1]
    half = rope_width // 2
    inverse = rope_base ** (-(np.arange(rope_width) % half) / half)
    inverse = jnp.asarray(inverse.reshape(1, -1), f32)

    w_value = jnp.swapaxes(w_absorb_value, 1, 2)

    def flat(g):
        return g.reshape(1, -1)

    ops = [
        tokens, routes, route_weights, flat(attn_gain), w_query, w_latent, w_absorb_key,
        w_rope_key.T, flat(latent_gain), cache_latent, cache_rope, flat(post_gain), flat(ffn_gain),
        flat(dense_gate_vector), w_exp_gate, w_exp_up, w_exp_down, w_dense_gate, w_dense_up,
        w_dense_down, flat(out_gain), inverse,
    ]
    lanes = -(-ep // 128) * 128
    dma = pltpu.SemaphoreType.DMA
    scratch = [pltpu.VMEM(a.shape, a.dtype) for a in ops]
    scratch += [
        pltpu.VMEM((tp,) + w_value.shape, bf16),
        pltpu.VMEM((tp,) + w_out.shape, bf16),
        dma((len(ops) + 2,)),
        pltpu.VMEM((tp, rows, width), bf16),
        pltpu.VMEM((tp, rows, heads_local, kv + rope_width), f32),
        pltpu.VMEM((tp, rows, heads_local, kv + rope_width), f32),
        pltpu.VMEM((tp, rows, w_latent.shape[1]), f32),
        pltpu.VMEM((tp, rows, w_latent.shape[1]), f32),
        pltpu.VMEM((kv // 128, rows * heads_local * tp, 128), f32),
        pltpu.VMEM((rows, lanes), f32),
        pltpu.VMEM((ep, rows, lanes), f32),
        pltpu.VMEM((rows, width), bf16),
        pltpu.VMEM((ep, rows, width), bf16),
        pltpu.VMEM((ep * rows, width), f32),
        pltpu.VMEM((ep, rows, width), bf16),
        pltpu.VMEM((ep, rows, width), bf16),
    ]
    scratch += [dma((tp,))] * 6 + [dma((tp, 3))] * 4 + [dma((ep,))] * 6
    anywhere = pl.BlockSpec(memory_space=pl.ANY)
    shapes = (
        jax.ShapeDtypeStruct((rows, width), bf16),
        jax.ShapeDtypeStruct((rows, kv), bf16),
        jax.ShapeDtypeStruct((rows, rope_width), bf16),
    )
    in_vmem = (pl.BlockSpec(memory_space=pltpu.VMEM),) * 3
    results = pl.pallas_call(
        functools.partial(kernel, ep, tp),
        out_shape=shapes,
        in_specs=[pl.BlockSpec(memory_space=pltpu.SMEM)] + [anywhere] * (len(ops) + 2),
        out_specs=in_vmem,
        scratch_shapes=scratch,
        compiler_params=pltpu.CompilerParams(
            collective_id=0, has_side_effects=True, vmem_limit_bytes=60 * 1024 * 1024
        ),
    )(lengths, *ops, w_value, w_out)
    return tuple(
        pl.pallas_call(hand_over, out_shape=shapes, in_specs=in_vmem, out_specs=in_vmem)(*results)
    )


def solution(mesh):
    placed = (
        P(("ep", "tp"), None),
        P(("ep", "tp")),
        P(("ep", "tp"), None, None),
        P(("ep", "tp"), None, None),
        P(),
        P(),
        P(),
        P(),
        P(),
        P(None, "tp"),
        P(),
        P(None, "tp"),
        P("tp", None, None),
        P("tp", None, None),
        P("tp", None),
        P(("ep", "tp"), None),
        P(("ep", "tp"), None),
        P("ep", None, None),
        P("ep", None, None),
        P("ep", None, None),
        P("ep", None),
        P("ep", None),
        P("ep", None),
        P(),
    )
    return jax.shard_map(
        shards,
        mesh=mesh,
        in_specs=placed,
        out_specs=(P(("ep", "tp"), None), P(("ep", "tp"), None), P(("ep", "tp"), None)),
        check_vma=False,
    )
```

profile of v0, /device:TPU:0, one launch (start us, length us, event | category | flops | bytes accessed | tf_op | source)
XLA Modules:
  0.0 32.4 jit_solution(6569844614076507895)
XLA Ops:
  0.6 30.5 %shard_map.256 = (bf16[4,1024]{1,0:T(4,128)(2,1)}, bf16[4,256]{1,0:T(4,128)(2,1)}, bf16[4,32]{1,0:T(4,128)(2,1)}) custom-call(s32[4]{0:T(128)} %refs_0_.1, bf16[4,1024]{1,0:T(4,128)(2,1)} %refs_1_.1, s32[4,6]{1,0:T(4,128)} %refs_2_.1, f32[4,6]{1,0:T(4,128)} %refs_3_.1, f32[1,1024]{1,0:T(1,128)} %bitcast.10, bf16[1024,384]{1,0:T(8,128)(2,1)} %refs_5_.1, ...), custom_call_target="tpu_custom_call" | custom-call | tf_op jit(solution)/shard_map/pallas_call | solution.py:381
  31.1 1.3 %shard_map.257 = (bf16[4,1024]{1,0:T(4,128)(2,1)}, bf16[4,256]{1,0:T(4,128)(2,1)}, bf16[4,32]{1,0:T(4,128)(2,1)}) custom-call(bf16[4,1024]{1,0:T(4,128)(2,1)} %get-tuple-element.6.refs_0_, bf16[4,256]{1,0:T(4,128)(2,1)} %get-tuple-element.7.refs_1_, bf16[4,32]{1,0:T(4,128)(2,1)} %get-tuple-element.8.refs_2_), custom_call_target="tpu_custom_call" | custom-call | tf_op jit(solution)/shard_map/pallas_call | solution.py:392
where the time goes:
time: 32.6 us; the launch traced here: 32.4 us
  Pallas kernels  31.8 us (98%)
  between operations  0.65 us (2%)
    pallas_call x1, Pallas kernels, shards(): pl.pallas_call(functools.partial(kernel, ep, tp), out_shape=shapes, in_sp...  30.5 us
    pallas_call x1, Pallas kernels, shards(): pl.pallas_call(hand_over, out_shape=shapes, in_specs=in_vmem, out_specs=i...  1.31 us

commit v1 on v0

--- a/solution.py
+++ b/solution.py
@@ -19,7 +19,7 @@
     "tokens", "routes", "rweights", "coef_gain", "w_query", "w_latent",
     "w_abk", "w_rope", "lat_gain", "cache", "rope", "post_gain",
     "ffn_gain", "dvec", "weg", "weu", "wed", "wdg",
-    "wdu", "wdd", "out_gain", "inverse",
+    "wdu", "wdd", "out_gain", "inverse", "lengths",
 )
 
 
@@ -46,11 +46,10 @@
 
 def kernel(ep, tp, *refs):
     n = len(NAMES)
-    lengths = refs[0]
-    hbm = dict(zip(NAMES, refs[1 : 1 + n]))
-    wv_hbm, wo_hbm = refs[1 + n : 3 + n]
-    out_ref, lat_ref, key_ref = refs[3 + n : 6 + n]
-    scratch = refs[6 + n :]
+    hbm = dict(zip(NAMES, refs[:n]))
+    wv_hbm, wo_hbm = refs[n : 2 + n]
+    out_ref, lat_ref, key_ref = refs[2 + n : 5 + n]
+    scratch = refs[5 + n :]
     v = dict(zip(NAMES, scratch[:n]))
     (
         wv, wo, load_sem, tokbuf, qsend, qbuf, latsend, latbuf, att, coef, coefbuf,
@@ -71,10 +70,10 @@
     loads = {}
     loads["wv"] = pltpu.make_async_copy(wv_hbm, wv.at[0], load_sem.at[n])
     loads["wo"] = pltpu.make_async_copy(wo_hbm, wo.at[0], load_sem.at[n + 1])
-    loads["wv"].start()
-    loads["wo"].start()
     for i, name in enumerate(NAMES):
         loads[name] = pltpu.make_async_copy(hbm[name], v[name], load_sem.at[i])
+    first = ("tokens", "wv", "wo", "routes", "rweights")
+    for name in first + tuple(name for name in NAMES if name not in first):
         loads[name].start()
 
     barrier = pltpu.get_barrier_semaphore()
@@ -87,27 +86,15 @@
             barrier, inc=1, device_id={"ep": lax.rem(me_e + k, ep)}, device_id_type=MESH
         )
 
-    for name in ("tokens", "routes", "rweights", "inverse"):
-        loads[name].wait()
-    lane = lax.broadcasted_iota(jnp.int32, coef.shape, 1)
-    total = jnp.zeros(coef.shape, f32)
-    routes = v["routes"][...]
-    rweights = v["rweights"][...]
-    for k in range(routes.shape[1]):
-        total = total + jnp.where(routes[:, k : k + 1] == lane, rweights[:, k : k + 1], 0.0)
-    coef[...] = total
-
     def tables(count, per):
         row = lax.broadcasted_iota(jnp.int32, (count, rope_width), 0) // per
         pos = jnp.zeros((count, rope_width), jnp.int32)
         for s in range(rows):
-            pos = jnp.where(row == s, lengths[s], pos)
+            pos = jnp.where(row == s, v["lengths"][:, s : s + 1], pos)
         angles = pos.astype(f32) * v["inverse"][...]
         return jnp.cos(angles), jnp.sin(angles)
 
-    cos_q, sin_q = tables(rows * heads, heads)
-    cos_k, sin_k = tables(rows, 1)
-
+    loads["tokens"].wait()
     pl.semaphore_wait(barrier, (tp - 1) + (ep - 1))
 
     def remote(src, dst, ss, rs, where):
@@ -118,8 +105,20 @@
 
     back_t = [lax.rem(me_t + tp - k, tp) for k in range(tp)]
     ahead_t = [lax.rem(me_t + k, tp) for k in range(tp)]
-    back_e = [lax.rem(me_e + ep - k, ep) for k in range(ep)]
-    ahead_e = [lax.rem(me_e + k, ep) for k in range(ep)]
+    others = range(ep - 1, 0, -1)
+    if ep & (ep - 1) == 0:
+        flips = [(1 - 2 * lax.rem(me_e // (1 << i), 2)) * (1 << i) for i in range(ep.bit_length() - 1)]
+        to_e = [me_e + sum(f for i, f in enumerate(flips) if k >> i & 1) for k in range(ep)]
+        slot, back_to = list(range(ep)), to_e
+    else:
+        to_e = [lax.rem(me_e + k, ep) for k in range(ep)]
+        slot = [(ep - k) % ep for k in range(ep)]
+        back_to = to_e
+    peers = pl.ds(1, ep - 1)
+
+    def all_of(buf, sem):
+        return pltpu.make_async_copy(buf.at[peers], buf.at[peers], sem)
+
     a_copies = [
         remote(v["tokens"], tokbuf.at[k], a_s.at[k], a_r.at[k], {"tp": back_t[k]})
         for k in range(1, tp)
@@ -160,11 +159,17 @@
     for group in w1:
         group[0].start()
         group[1].start()
-    c_copies = [
-        remote(coef, coefbuf.at[k], c_s.at[k], c_r.at[k], {"ep": back_e[k]}) for k in range(1, ep)
-    ]
-    for c in c_copies:
-        c.start()
+    loads["routes"].wait()
+    loads["rweights"].wait()
+    lane = lax.broadcasted_iota(jnp.int32, coef.shape, 1)
+    total = jnp.zeros(coef.shape, f32)
+    routes = v["routes"][...]
+    rweights = v["rweights"][...]
+    for k in range(routes.shape[1]):
+        total = total + jnp.where(routes[:, k : k + 1] == lane, rweights[:, k : k + 1], 0.0)
+    coef[...] = total
+    for k in others:
+        remote(coef, coefbuf.at[slot[k]], c_s, c_r, {"ep": to_e[k]}).start()
 
     tokens = v["tokens"][...].astype(f32)
     for c in a_copies:
@@ -204,6 +209,10 @@
         c.start()
     for group in w1:
         group[2].start()
+    loads["lengths"].wait()
+    loads["inverse"].wait()
+    cos_q, sin_q = tables(rows * heads, heads)
+    cos_k, sin_k = tables(rows, 1)
     loads["w_rope"].wait()
     raw_key = dot_t(hidden, v["w_rope"][...])[0:rows]
     new_key = (raw_key * cos_k + swap_halves(raw_key) * sin_k).astype(bf16)
@@ -228,25 +237,43 @@
     q_lat = q_all[:, 0:kv]
     q_raw = q_all[:, kv : kv + rope_width]
     q_rot = (q_raw * cos_q + swap_halves(q_raw) * sin_q).astype(bf16)
-    position = lax.broadcasted_iota(jnp.int32, (heads, v["cache"].shape[1]), 1)
+    def spread(block):
+        return jnp.concatenate(
+            [jnp.broadcast_to(block[s : s + 1], (heads, block.shape[1])) for s in range(rows)],
+            axis=0,
+        )
+
+    depth_c = v["cache"].shape[1]
+    lat_q = spread(lat_f)
+    own = (
+        jnp.sum(q_lat * lat_q, axis=1, keepdims=True)
+        + jnp.sum(q_rot.astype(f32) * spread(key_f), axis=1, keepdims=True)
+    ) * scaling
+    q_rot = q_rot.astype(f32)
+    blocks = [slice(s * heads, (s + 1) * heads) for s in range(rows)]
+    scores = jnp.concatenate(
+        [
+            dot_t(q_lat[b].astype(bf16), v["cache"][s]) + dot(q_rot[b].astype(bf16), v["rope"][s])
+            for s, b in enumerate(blocks)
+        ],
+        axis=0,
+    )
+    seq = lax.broadcasted_iota(jnp.int32, (rows * heads, 1), 0) // heads
+    limit = jnp.zeros((rows * heads, 1), jnp.int32)
     for s in range(rows):
-        ql = q_lat[s * heads : (s + 1) * heads]
-        qr = q_rot[s * heads : (s + 1) * heads]
-        own = (
-            jnp.sum(ql * lat_f[s : s + 1], axis=1, keepdims=True)
-            + jnp.sum(qr.astype(f32) * key_f[s : s + 1], axis=1, keepdims=True)
-        ) * scaling
-        scores = (dot_t(ql.astype(bf16), v["cache"][s]) + dot(qr, v["rope"][s])) * scaling
-        scores = jnp.where(position < lengths[s], scores, negative)
-        top = jnp.maximum(jnp.max(scores, axis=1, keepdims=True), own)
-        weights = jnp.exp(scores - top)
-        own_weight = jnp.exp(own - top)
-        share = 1.0 / (jnp.sum(weights, axis=1, keepdims=True) + own_weight)
-        probabilities = (weights * share).astype(bf16)
-        own_prob = (own_weight * share).astype(bf16).astype(f32)
-        attended = dot(probabilities, v["cache"][s]) + own_prob * lat_f[s : s + 1]
-        for j in range(kv // 128):
-            att[j, s * heads : (s + 1) * heads] = attended[:, j * 128 : (j + 1) * 128]
+        limit = jnp.where(seq == s, v["lengths"][:, s : s + 1], limit)
+    position = lax.broadcasted_iota(jnp.int32, (rows * heads, depth_c), 1)
+    scores = jnp.where(position < limit, scores * scaling, negative)
+    top = jnp.maximum(jnp.max(scores, axis=1, keepdims=True), own)
+    weights = jnp.exp(scores - top)
+    own_weight = jnp.exp(own - top)
+    share = 1.0 / (jnp.sum(weights, axis=1, keepdims=True) + own_weight)
+    attended = jnp.concatenate(
+        [dot(weights[b].astype(bf16), v["cache"][s]) for s, b in enumerate(blocks)], axis=0
+    )
+    attended = (attended + own_weight * lat_q) * share
+    for j in range(kv // 128):
+        att[j] = attended[:, j * 128 : (j + 1) * 128]
     for group, forward in zip(w1, w2):
         group[2].wait_recv()
         forward[2].start()
@@ -267,26 +294,21 @@
     residual = (tokens + norm(mixed) * v["post_gain"][...]).astype(bf16).astype(f32)
     ffn_in = (norm(residual) * v["ffn_gain"][...]).astype(bf16)
     xown[...] = ffn_in
-    x_copies = [
-        remote(xown, xbuf.at[k], x_s.at[k], x_r.at[k], {"ep": back_e[k]}) for k in range(1, ep)
-    ]
-    for c in x_copies:
-        c.start()
+    for k in others:
+        remote(xown, xbuf.at[slot[k]], x_s, x_r, {"ep": to_e[k]}).start()
     for name in ("dvec", "weg", "weu", "wed", "wdg", "wdu", "wdd", "out_gain"):
         loads[name].wait()
-    lane_own = lax.broadcasted_iota(jnp.int32, coef.shape, 1) == me_e
+    lane_own = lax.broadcasted_iota(jnp.int32, (ep * rows, coef.shape[1]), 1) == me_e
 
     def own_weight_of(block):
         return jnp.sum(jnp.where(lane_own, block, 0.0), axis=1, keepdims=True)
 
-    route_parts = [own_weight_of(coef[...])]
-    for k in range(1, ep):
-        c_copies[k - 1].wait_recv()
-        route_parts.append(own_weight_of(coefbuf[k]))
-    route_w = jnp.concatenate(route_parts, axis=0)
+    all_of(coefbuf, c_r).wait()
+    route_w = own_weight_of(
+        jnp.concatenate([coef[...]] + [coefbuf[k] for k in range(1, ep)], axis=0)
+    )
     xrows[0:rows] = ffn_in.astype(f32)
-    for k in range(1, ep):
-        x_copies[k - 1].wait_recv()
+    all_of(xbuf, x_r).wait()
     for k in range(1, ep):
         xrows[k * rows : (k + 1) * rows] = xbuf[k].astype(f32)
     x_f = xrows[...]
@@ -299,23 +321,21 @@
     )
     for k in range(1, ep):
         psend[k] = partial[k * rows : (k + 1) * rows].astype(bf16)
-    p_copies = [
-        remote(psend.at[k], pbuf.at[ep - k], p_s.at[k], p_r.at[ep - k], {"ep": ahead_e[k]})
-        for k in range(1, ep)
-    ]
-    for c in p_copies:
-        c.start()
+    for k in others:
+        remote(psend.at[k], pbuf.at[k], p_s, p_r, {"ep": back_to[k]}).start()
     combined = partial[0:rows]
+    all_of(pbuf, p_r).wait()
     for k in range(1, ep):
-        p_copies[k - 1].wait_recv()
-    for k in range(1, ep):
-        combined = combined + pbuf[ep - k].astype(f32)
+        combined = combined + pbuf[k].astype(f32)
     out_ref[...] = (residual + norm(combined) * v["out_gain"][...]).astype(bf16)
-    for c in a_copies + q_copies + l_copies + c_copies + x_copies + p_copies:
+    for c in a_copies + q_copies + l_copies:
         c.wait_send()
     for group in w1 + w2:
         for c in group:
             c.wait_send()
+    all_of(coefbuf, c_s).wait()
+    all_of(xbuf, x_s).wait()
+    all_of(psend, p_s).wait()
 
 
 def hand_over(*refs):
@@ -347,7 +367,7 @@
         tokens, routes, route_weights, flat(attn_gain), w_query, w_latent, w_absorb_key,
         w_rope_key.T, flat(latent_gain), cache_latent, cache_rope, flat(post_gain), flat(ffn_gain),
         flat(dense_gate_vector), w_exp_gate, w_exp_up, w_exp_down, w_dense_gate, w_dense_up,
-        w_dense_down, flat(out_gain), inverse,
+        w_dense_down, flat(out_gain), inverse, flat(lengths),
     ]
     lanes = -(-ep // 128) * 128
     dma = pltpu.SemaphoreType.DMA
@@ -370,7 +390,7 @@
         pltpu.VMEM((ep, rows, width), bf16),
         pltpu.VMEM((ep, rows, width), bf16),
     ]
-    scratch += [dma((tp,))] * 6 + [dma((tp, 3))] * 4 + [dma((ep,))] * 6
+    scratch += [dma((tp,))] * 6 + [dma((tp, 3))] * 4 + [dma] * 6
     anywhere = pl.BlockSpec(memory_space=pl.ANY)
     shapes = (
         jax.ShapeDtypeStruct((rows, width), bf16),
@@ -381,13 +401,13 @@
     results = pl.pallas_call(
         functools.partial(kernel, ep, tp),
         out_shape=shapes,
-        in_specs=[pl.BlockSpec(memory_space=pltpu.SMEM)] + [anywhere] * (len(ops) + 2),
+        in_specs=[anywhere] * (len(ops) + 2),
         out_specs=in_vmem,
         scratch_shapes=scratch,
         compiler_params=pltpu.CompilerParams(
             collective_id=0, has_side_effects=True, vmem_limit_bytes=60 * 1024 * 1024
         ),
-    )(lengths, *ops, w_value, w_out)
+    )(*ops, w_value, w_out)
     return tuple(
         pl.pallas_call(hand_over, out_shape=shapes, in_specs=in_vmem, out_specs=in_vmem)(*results)
     )

time: 32.6 us -> 31.5 us (0.966)
  Pallas kernels: 31.8 us -> 30.6 us
    pallas_call x1, Pallas kernels: 30.5 us -> 29.3 us  [shards(): pl.pallas_call(functools.partial(kernel, ep, tp), out_shape=shapes, in_sp...]
where the time goes in v1:
time: 31.5 us; the launch traced here: 31.3 us
  Pallas kernels  30.6 us (97%)
  between operations  0.65 us (2%)
    pallas_call x1, Pallas kernels, shards(): pl.pallas_call(functools.partial(kernel, ep, tp), out_shape=shapes, in_sp...  29.3 us
    pallas_call x1, Pallas kernels, shards(): pl.pallas_call(hand_over, out_shape=shapes, in_specs=in_vmem, out_specs=i...  1.31 us

profile of v1, /device:TPU:0, one launch (start us, length us, event | category | flops | bytes accessed | tf_op | source)
XLA Modules:
  0.0 31.3 jit_solution(17646759231038077830)
XLA Ops:
  0.6 29.3 %shard_map.256 = (bf16[4,1024]{1,0:T(4,128)(2,1)}, bf16[4,256]{1,0:T(4,128)(2,1)}, bf16[4,32]{1,0:T(4,128)(2,1)}) custom-call(bf16[4,1024]{1,0:T(4,128)(2,1)} %refs_0_.1, s32[4,6]{1,0:T(4,128)} %refs_1_.1, f32[4,6]{1,0:T(4,128)} %refs_2_.1, f32[1,1024]{1,0:T(1,128)} %bitcast.11, bf16[1024,384]{1,0:T(8,128)(2,1)} %refs_4_.1, bf16[1024,128]{1,0:T(8,128)(2,1)} %refs_5_.1, ...), custom_call_target="tpu_custom_call" | custom-call | tf_op jit(solution)/shard_map/pallas_call | solution.py:401
  30.0 1.3 %shard_map.257 = (bf16[4,1024]{1,0:T(4,128)(2,1)}, bf16[4,256]{1,0:T(4,128)(2,1)}, bf16[4,32]{1,0:T(4,128)(2,1)}) custom-call(bf16[4,1024]{1,0:T(4,128)(2,1)} %get-tuple-element.6.refs_0_, bf16[4,256]{1,0:T(4,128)(2,1)} %get-tuple-element.7.refs_1_, bf16[4,32]{1,0:T(4,128)(2,1)} %get-tuple-element.8.refs_2_), custom_call_target="tpu_custom_call" | custom-call | tf_op jit(solution)/shard_map/pallas_call | solution.py:412

commit v2 on v1

--- a/solution.py
+++ b/solution.py
@@ -54,7 +54,7 @@
     (
         wv, wo, load_sem, tokbuf, qsend, qbuf, latsend, latbuf, att, coef, coefbuf,
         xown, xbuf, xrows, psend, pbuf,
-        a_s, a_r, q_s, q_r, l_s, l_r, w1_s, w1_r, w2_s, w2_r, c_s, c_r, x_s, x_r, p_s, p_r,
+        a_s, a_r, q_s, q_r, l_s, l_r, wv_sem, wx_s, wf_s, wx_r, wf_r, c_s, c_r, x_s, x_r, p_s, p_r,
     ) = scratch[n:]
     rows, width = v["tokens"].shape
     heads_local, nope, kv = v["w_abk"].shape
@@ -81,6 +81,9 @@
         pl.semaphore_signal(
             barrier, inc=1, device_id={"tp": lax.rem(me_t + k, tp)}, device_id_type=MESH
         )
+        pl.semaphore_signal(
+            barrier, inc=1, device_id={"tp": lax.rem(me_t + k, tp), "ep": sibling}, device_id_type=MESH
+        )
     for k in range(1, ep):
         pl.semaphore_signal(
             barrier, inc=1, device_id={"ep": lax.rem(me_e + k, ep)}, device_id_type=MESH
@@ -95,7 +98,7 @@
         return jnp.cos(angles), jnp.sin(angles)
 
     loads["tokens"].wait()
-    pl.semaphore_wait(barrier, (tp - 1) + (ep - 1))
+    pl.semaphore_wait(barrier, 2 * (tp - 1) + (ep - 1))
 
     def remote(src, dst, ss, rs, where):
         return pltpu.make_async_remote_copy(
@@ -120,45 +123,72 @@
         return pltpu.make_async_copy(buf.at[peers], buf.at[peers], sem)
 
     a_copies = [
-        remote(v["tokens"], tokbuf.at[k], a_s.at[k], a_r.at[k], {"tp": back_t[k]})
+        remote(v["tokens"], tokbuf.at[k], a_s.at[k], a_r.at[k], {"tp": back_t[k], "ep": sibling})
         for k in range(1, tp)
     ]
     for c in a_copies:
         c.start()
     half_h = heads_local // 2
     depth = wo.shape[1]
-    quarter = depth // 8
-    part = depth // 16
-
-    def pieces(k):
-        start = core * (4 * quarter)
-        early = pl.ds(pl.multiple_of(start, quarter), 2 * quarter - part)
-        late = pl.ds(pl.multiple_of(start + 2 * quarter - part, part), 2 * quarter + part)
-        return (
-            wv.at[k, pl.ds(core * half_h, half_h)],
-            wo.at[k, early],
-            wo.at[k, late],
-        )
-
-    w1 = [
-        [
-            remote(src, dst, w1_s.at[k, i], w1_r.at[k, i], {"tp": back_t[k]})
-            for i, (src, dst) in enumerate(zip(pieces(0), pieces(k)))
-        ]
-        for k in range(1, tp)
-    ]
-    w2 = [
-        [
-            remote(dst, dst, w2_s.at[k, i], w2_r.at[k, i], {"ep": sibling})
-            for i, dst in enumerate(pieces(k))
-        ]
-        for k in range(1, tp)
-    ]
-    loads['wv'].wait()
-    loads['wo'].wait()
-    for group in w1:
-        group[0].start()
-        group[1].start()
+    eighth = depth // 8
+    step = max(16, eighth // 2)
+    member = lax.rem(me_e, 4)
+
+    def wo_rows(k, start, size):
+        return wo.at[k, pl.ds(pl.multiple_of(start, 16), size)]
+
+    shared = [(member * eighth + i, step) for i in range(0, eighth, step)]
+    local = [
+        (depth // 2 + core * (2 * eighth) + i, size)
+        for i, size in ((0, eighth), (eighth, step)) + (((eighth + step, step),) if step < eighth else ())
+    ]
+    n_s, n_l = len(shared), len(local)
+    halves = pl.ds(core * half_h, half_h)
+    to_mate = {
+        j: me_e + sum((1 - 2 * lax.rem(me_e // (1 << i), 2)) * (1 << i) for i in range(2) if j >> i & 1)
+        for j in (1, 2, 3)
+    }
+    x_wv, x_sh, x_lo, f_wv, f_sh, f_lo = [], [], [], [], [], []
+    for k in range(1, tp):
+        away = {"tp": back_t[k]}
+        mine = wv.at[k, halves]
+        x_wv.append(remote(wv.at[0, halves], mine, wv_sem.at[0], wv_sem.at[k], away))
+        f_wv.append(remote(mine, mine, wv_sem.at[tp], wv_sem.at[tp + k], {"ep": sibling}))
+        x_sh.append(
+            [
+                remote(wo_rows(0, *r), wo_rows(k, *r), wx_s.at[k], wx_r.at[k, i], away)
+                for i, r in enumerate(shared)
+            ]
+        )
+        x_lo.append(
+            [
+                remote(wo_rows(0, *r), wo_rows(k, *r), wx_s.at[k], wx_r.at[k, n_s + i], away)
+                for i, r in enumerate(local)
+            ]
+        )
+        f_sh.append(
+            [
+                [
+                    remote(wo_rows(k, *r), wo_rows(k, *r), wf_s.at[k], wf_r.at[k, 3 * i + j - 1], {"ep": to_mate[j]})
+                    for j in (2, 3, 1)
+                ]
+                for i, r in enumerate(shared)
+            ]
+        )
+        f_lo.append(
+            [
+                remote(wo_rows(k, *r), wo_rows(k, *r), wf_s.at[k], wf_r.at[k, 3 * n_s + i], {"ep": sibling})
+                for i, r in enumerate(local)
+            ]
+        )
+    loads["wo"].wait()
+    for k in range(tp - 1):
+        for c in x_sh[k]:
+            c.start()
+    loads["wv"].wait()
+    for k in range(tp - 1):
+        x_wv[k].start()
+        x_lo[k][0].start()
     loads["routes"].wait()
     loads["rweights"].wait()
     lane = lax.broadcasted_iota(jnp.int32, coef.shape, 1)
@@ -198,17 +228,18 @@
         latsend[k] = latent_part[k * rows : (k + 1) * rows]
     latbuf[me_t] = latent_part[0:rows]
     q_copies = [
-        remote(qsend.at[k], qbuf.at[tp - k], q_s.at[k], q_r.at[tp - k], {"tp": ahead_t[k]})
+        remote(qsend.at[k], qbuf.at[tp - k], q_s.at[k], q_r.at[tp - k], {"tp": ahead_t[k], "ep": sibling})
         for k in range(1, tp)
     ]
     l_copies = [
-        remote(latsend.at[k], latbuf.at[me_t], l_s.at[k], l_r.at[tp - k], {"tp": ahead_t[k]})
+        remote(latsend.at[k], latbuf.at[me_t], l_s.at[k], l_r.at[tp - k], {"tp": ahead_t[k], "ep": sibling})
         for k in range(1, tp)
     ]
     for c in q_copies + l_copies:
         c.start()
-    for group in w1:
-        group[2].start()
+    for k in range(tp - 1):
+        for c in x_lo[k][1:]:
+            c.start()
     loads["lengths"].wait()
     loads["inverse"].wait()
     cos_q, sin_q = tables(rows * heads, heads)
@@ -217,15 +248,19 @@
     raw_key = dot_t(hidden, v["w_rope"][...])[0:rows]
     new_key = (raw_key * cos_k + swap_halves(raw_key) * sin_k).astype(bf16)
     key_ref[...] = new_key
+    for k in range(tp - 1):
+        for c, forward in zip(x_sh[k], f_sh[k]):
+            c.wait_recv()
+            for f in forward:
+                f.start()
     loads["cache"].wait()
     loads["rope"].wait()
     loads["lat_gain"].wait()
     for c in q_copies + l_copies:
         c.wait_recv()
-    for i in (0, 1):
-        for group, forward in zip(w1, w2):
-            group[i].wait_recv()
-            forward[i].start()
+    for k in range(tp - 1):
+        x_wv[k].wait_recv()
+        f_wv[k].start()
     latent = jnp.concatenate([latbuf[t] for t in range(tp)], axis=1)
     new_latent = (norm(latent) * v["lat_gain"][...]).astype(bf16)
     lat_ref[...] = new_latent
@@ -274,21 +309,28 @@
     attended = (attended + own_weight * lat_q) * share
     for j in range(kv // 128):
         att[j] = attended[:, j * 128 : (j + 1) * 128]
-    for group, forward in zip(w1, w2):
-        group[2].wait_recv()
-        forward[2].start()
-    mixed = jnp.zeros((rows, width), f32)
+    for k in range(tp - 1):
+        for c, forward in zip(x_lo[k], f_lo[k]):
+            c.wait_recv()
+            forward.start()
+    outs = []
     for k in range(tp):
         if k > 0:
-            for c in w2[k - 1]:
-                c.wait_recv()
+            f_wv[k - 1].wait_recv()
         parts = []
         for h in range(heads_local):
             chosen = pl.ds(k * heads_local + h, rows, stride=heads)
             picked = jnp.concatenate([att[j, chosen, :] for j in range(kv // 128)], axis=1)
             parts.append(dot_t(picked.astype(bf16), wv[k, h]))
-        head_out = jnp.concatenate(parts, axis=1).astype(bf16)
-        mixed = mixed + dot(head_out, wo[k]).astype(bf16).astype(f32)
+        outs.append(jnp.concatenate(parts, axis=1).astype(bf16))
+    mixed = dot(outs[0], wo[0]).astype(bf16).astype(f32)
+    for k in range(1, tp):
+        for forward in f_sh[k - 1]:
+            for f in forward:
+                f.wait_recv()
+        for f in f_lo[k - 1]:
+            f.wait_recv()
+        mixed = mixed + dot(outs[k], wo[k]).astype(bf16).astype(f32)
     loads["post_gain"].wait()
     loads["ffn_gain"].wait()
     residual = (tokens + norm(mixed) * v["post_gain"][...]).astype(bf16).astype(f32)
@@ -330,9 +372,16 @@
     out_ref[...] = (residual + norm(combined) * v["out_gain"][...]).astype(bf16)
     for c in a_copies + q_copies + l_copies:
         c.wait_send()
-    for group in w1 + w2:
-        for c in group:
-            c.wait_send()
+    for k in range(tp - 1):
+        pltpu.make_async_copy(
+            wo_rows(k + 1, 0, 3 * eighth), wo_rows(k + 1, 0, 3 * eighth), wx_s.at[k + 1]
+        ).wait()
+        pltpu.make_async_copy(
+            wo_rows(k + 1, 0, 5 * eighth), wo_rows(k + 1, 0, 5 * eighth), wf_s.at[k + 1]
+        ).wait()
+    every = wv.at[pl.ds(1, tp - 1), halves]
+    pltpu.make_async_copy(every, every, wv_sem.at[0]).wait()
+    pltpu.make_async_copy(every, every, wv_sem.at[tp]).wait()
     all_of(coefbuf, c_s).wait()
     all_of(xbuf, x_s).wait()
     all_of(psend, p_s).wait()
@@ -390,7 +439,8 @@
         pltpu.VMEM((ep, rows, width), bf16),
         pltpu.VMEM((ep, rows, width), bf16),
     ]
-    scratch += [dma((tp,))] * 6 + [dma((tp, 3))] * 4 + [dma] * 6
+    scratch += [dma((tp,))] * 6 + [dma((2 * tp,)), dma((tp,)), dma((tp,)), dma((tp, 5)), dma((tp, 9))]
+    scratch += [dma] * 6
     anywhere = pl.BlockSpec(memory_space=pl.ANY)
     shapes = (
         jax.ShapeDtypeStruct((rows, width), bf16),
@@ -400,7 +450,7 @@
     in_vmem = (pl.BlockSpec(memory_space=pltpu.VMEM),) * 3
     results = pl.pallas_call(
         functools.partial(kernel, ep, tp),
-        out_shape=shapes,
+        out_shape=tuple(pltpu.VMEM(o.shape, o.dtype) for o in shapes),
         in_specs=[anywhere] * (len(ops) + 2),
         out_specs=in_vmem,
         scratch_shapes=scratch,
@@ -409,7 +459,7 @@
         ),
     )(*ops, w_value, w_out)
     return tuple(
-        pl.pallas_call(hand_over, out_shape=shapes, in_specs=in_vmem, out_specs=in_vmem)(*results)
+        pl.pallas_call(hand_over, out_shape=shapes, in_specs=in_vmem, out_specs=in_vmem)(*[pltpu.with_memory_space_constraint(r, pltpu.VMEM) for r in results])
     )
 
 

time: 31.5 us -> 28.9 us (0.917)
  Pallas kernels: 30.6 us -> 28 us
    pallas_call x1, Pallas kernels: 29.3 us -> 27.4 us  [shards(): pl.pallas_call(functools.partial(kernel, ep, tp), out_shape=tuple((pltpu....]
    pallas_call x1, Pallas kernels: 1.31 us -> 0.61 us  [shards(): pl.pallas_call(hand_over, out_shape=shapes, in_specs=in_vmem, out_specs=i...]
where the time goes in v2:
time: 28.9 us; the launch traced here: 28.7 us
  Pallas kernels  28 us (97%)
  between operations  0.65 us (2%)
    pallas_call x1, Pallas kernels, shards(): pl.pallas_call(functools.partial(kernel, ep, tp), out_shape=tuple((pltpu....  27.4 us
    pallas_call x1, Pallas kernels, shards(): pl.pallas_call(hand_over, out_shape=shapes, in_specs=in_vmem, out_specs=i...  0.61 us

profile of v2, /device:TPU:0, one launch (start us, length us, event | category | flops | bytes accessed | tf_op | source)
XLA Modules:
  0.0 28.7 jit_solution(14775599157792803928)
XLA Ops:
  0.6 27.4 %shard_map.256 = (bf16[4,1024]{1,0:T(4,128)(2,1)S(1)}, bf16[4,256]{1,0:T(4,128)(2,1)S(1)}, bf16[4,32]{1,0:T(4,128)(2,1)S(1)}) custom-call(bf16[4,1024]{1,0:T(4,128)(2,1)} %refs_0_.1, s32[4,6]{1,0:T(4,128)} %refs_1_.1, f32[4,6]{1,0:T(4,128)} %refs_2_.1, f32[1,1024]{1,0:T(1,128)} %bitcast.11, bf16[1024,384]{1,0:T(8,128)(2,1)} %refs_4_.1, ...), custom_call_target="tpu_custom_call" | custom-call | tf_op jit(solution)/shard_map/pallas_call | solution.py:451
  28.1 0.6 %shard_map.257 = (bf16[4,1024]{1,0:T(4,128)(2,1)}, bf16[4,256]{1,0:T(4,128)(2,1)}, bf16[4,32]{1,0:T(4,128)(2,1)}) custom-call(bf16[4,1024]{1,0:T(4,128)(2,1)S(1)} %get-tuple-element.6.refs_0_, bf16[4,256]{1,0:T(4,128)(2,1)S(1)} %get-tuple-element.7.refs_1_, bf16[4,32]{1,0:T(4,128)(2,1)S(1)} %get-tuple-element.8.refs_2_), custom_call_target="tpu_custom_call" | custom-call | tf_op jit(solution)/shard_map/pallas_call | solution.py:462

commit v3 on v2

--- a/solution.py
+++ b/solution.py
@@ -54,7 +54,7 @@
     (
         wv, wo, load_sem, tokbuf, qsend, qbuf, latsend, latbuf, att, coef, coefbuf,
         xown, xbuf, xrows, psend, pbuf,
-        a_s, a_r, q_s, q_r, l_s, l_r, wv_sem, wx_s, wf_s, wx_r, wf_r, c_s, c_r, x_s, x_r, p_s, p_r,
+        a_s, a_r, q_s, q_r, l_s, l_r, wv_sem, wx_s, wf_s, wx_r, wf_r, known, c_s, c_r, x_s, x_r, p_s, p_r,
     ) = scratch[n:]
     rows, width = v["tokens"].shape
     heads_local, nope, kv = v["w_abk"].shape
@@ -84,10 +84,36 @@
         pl.semaphore_signal(
             barrier, inc=1, device_id={"tp": lax.rem(me_t + k, tp), "ep": sibling}, device_id_type=MESH
         )
-    for k in range(1, ep):
-        pl.semaphore_signal(
-            barrier, inc=1, device_id={"ep": lax.rem(me_e + k, ep)}, device_id_type=MESH
-        )
+    quads = ep // 4
+    quad = me_e // 4
+
+    def mate(j):
+        return me_e + sum(
+            (1 - 2 * lax.rem(me_e // (1 << i), 2)) * (1 << i) for i in range(2) if j >> i & 1
+        )
+
+    def greet(sem, where):
+        pl.semaphore_signal(sem, inc=1, device_id=where, device_id_type=MESH)
+
+    def greet_line(sem, reach):
+        @pl.when(quad >= reach)
+        def _():
+            greet(sem, {"ep": me_e - 4 * reach})
+
+        @pl.when(quad < quads - reach)
+        def _():
+            greet(sem, {"ep": me_e + 4 * reach})
+
+    def in_line(reach):
+        return (quad >= reach).astype(jnp.int32) + (quad < quads - reach).astype(jnp.int32)
+
+    def greet_mates(sem):
+        for j in (2, 3, 1):
+            greet(sem, {"ep": mate(j)})
+
+    stages = (quads - 1).bit_length()
+    greet_mates(barrier)
+    greet_line(barrier, 1)
 
     def tables(count, per):
         row = lax.broadcasted_iota(jnp.int32, (count, rope_width), 0) // per
@@ -98,7 +124,7 @@
         return jnp.cos(angles), jnp.sin(angles)
 
     loads["tokens"].wait()
-    pl.semaphore_wait(barrier, 2 * (tp - 1) + (ep - 1))
+    pl.semaphore_wait(barrier, 2 * (tp - 1) + 3 + in_line(1))
 
     def remote(src, dst, ss, rs, where):
         return pltpu.make_async_remote_copy(
@@ -128,6 +154,7 @@
     ]
     for c in a_copies:
         c.start()
+    greet_line(known.at[0], 1)
     half_h = heads_local // 2
     depth = wo.shape[1]
     eighth = depth // 8
@@ -144,10 +171,6 @@
     ]
     n_s, n_l = len(shared), len(local)
     halves = pl.ds(core * half_h, half_h)
-    to_mate = {
-        j: me_e + sum((1 - 2 * lax.rem(me_e // (1 << i), 2)) * (1 << i) for i in range(2) if j >> i & 1)
-        for j in (1, 2, 3)
-    }
     x_wv, x_sh, x_lo, f_wv, f_sh, f_lo = [], [], [], [], [], []
     for k in range(1, tp):
         away = {"tp": back_t[k]}
@@ -169,7 +192,7 @@
         f_sh.append(
             [
                 [
-                    remote(wo_rows(k, *r), wo_rows(k, *r), wf_s.at[k], wf_r.at[k, 3 * i + j - 1], {"ep": to_mate[j]})
+                    remote(wo_rows(k, *r), wo_rows(k, *r), wf_s.at[k], wf_r.at[k, 3 * i + j - 1], {"ep": mate(j)})
                     for j in (2, 3, 1)
                 ]
                 for i, r in enumerate(shared)
@@ -198,9 +221,6 @@
     for k in range(routes.shape[1]):
         total = total + jnp.where(routes[:, k : k + 1] == lane, rweights[:, k : k + 1], 0.0)
     coef[...] = total
-    for k in others:
-        remote(coef, coefbuf.at[slot[k]], c_s, c_r, {"ep": to_e[k]}).start()
-
     tokens = v["tokens"][...].astype(f32)
     for c in a_copies:
         c.wait_recv()
@@ -240,6 +260,9 @@
     for k in range(tp - 1):
         for c in x_lo[k][1:]:
             c.start()
+    pl.semaphore_wait(known.at[0], in_line(1))
+    if stages > 1:
+        greet_line(known.at[1], 2)
     loads["lengths"].wait()
     loads["inverse"].wait()
     cos_q, sin_q = tables(rows * heads, heads)
@@ -261,6 +284,11 @@
     for k in range(tp - 1):
         x_wv[k].wait_recv()
         f_wv[k].start()
+    for stage in range(1, stages):
+        pl.semaphore_wait(known.at[stage], in_line(1 << stage))
+        if stage + 1 < stages:
+            greet_line(known.at[stage + 1], 2 << stage)
+    greet_mates(known.at[stages])
     latent = jnp.concatenate([latbuf[t] for t in range(tp)], axis=1)
     new_latent = (norm(latent) * v["lat_gain"][...]).astype(bf16)
     lat_ref[...] = new_latent
@@ -309,6 +337,9 @@
     attended = (attended + own_weight * lat_q) * share
     for j in range(kv // 128):
         att[j] = attended[:, j * 128 : (j + 1) * 128]
+    pl.semaphore_wait(known.at[stages], 3)
+    for k in others:
+        remote(coef, coefbuf.at[slot[k]], c_s, c_r, {"ep": to_e[k]}).start()
     for k in range(tp - 1):
         for c, forward in zip(x_lo[k], f_lo[k]):
             c.wait_recv()
@@ -440,6 +471,7 @@
         pltpu.VMEM((ep, rows, width), bf16),
     ]
     scratch += [dma((tp,))] * 6 + [dma((2 * tp,)), dma((tp,)), dma((tp,)), dma((tp, 5)), dma((tp, 9))]
+    scratch += [pltpu.SemaphoreType.REGULAR(((ep // 4 - 1).bit_length() + 1,))]
     scratch += [dma] * 6
     anywhere = pl.BlockSpec(memory_space=pl.ANY)
     shapes = (

time: 28.9 us -> 27.8 us (0.962)
  Pallas kernels: 28 us -> 26.9 us
    pallas_call x1, Pallas kernels: 27.4 us -> 26.3 us  [shards(): pl.pallas_call(functools.partial(kernel, ep, tp), out_shape=tuple((pltpu....]
where the time goes in v3:
time: 27.8 us; the launch traced here: 27.6 us
  Pallas kernels  26.9 us (97%)
  between operations  0.65 us (2%)
    pallas_call x1, Pallas kernels, shards(): pl.pallas_call(functools.partial(kernel, ep, tp), out_shape=tuple((pltpu....  26.3 us
    pallas_call x1, Pallas kernels, shards(): pl.pallas_call(hand_over, out_shape=shapes, in_specs=in_vmem, out_specs=i...  0.61 us

profile of v3, /device:TPU:0, one launch (start us, length us, event | category | flops | bytes accessed | tf_op | source)
XLA Modules:
  0.0 27.6 jit_solution(6898364637529769366)
XLA Ops:
  0.6 26.3 %shard_map.256 = (bf16[4,1024]{1,0:T(4,128)(2,1)S(1)}, bf16[4,256]{1,0:T(4,128)(2,1)S(1)}, bf16[4,32]{1,0:T(4,128)(2,1)S(1)}) custom-call(bf16[4,1024]{1,0:T(4,128)(2,1)} %refs_0_.1, s32[4,6]{1,0:T(4,128)} %refs_1_.1, f32[4,6]{1,0:T(4,128)} %refs_2_.1, f32[1,1024]{1,0:T(1,128)} %bitcast.11, bf16[1024,384]{1,0:T(8,128)(2,1)} %refs_4_.1, ...), custom_call_target="tpu_custom_call" | custom-call | tf_op jit(solution)/shard_map/pallas_call | solution.py:483
  27.0 0.6 %shard_map.257 = (bf16[4,1024]{1,0:T(4,128)(2,1)}, bf16[4,256]{1,0:T(4,128)(2,1)}, bf16[4,32]{1,0:T(4,128)(2,1)}) custom-call(bf16[4,1024]{1,0:T(4,128)(2,1)S(1)} %get-tuple-element.6.refs_0_, bf16[4,256]{1,0:T(4,128)(2,1)S(1)} %get-tuple-element.7.refs_1_, bf16[4,32]{1,0:T(4,128)(2,1)S(1)} %get-tuple-element.8.refs_2_), custom_call_target="tpu_custom_call" | custom-call | tf_op jit(solution)/shard_map/pallas_call | solution.py:494
